TPU v7x, 256 devices: a whole 4x4x8 slice. The times are simulated.
256 devices in a mesh: fs: 32 (over z, x), tp: 8 (over y, core).
Axes of the slice: x: 4, y: 4, z: 8, core: 2. Of those that a mesh axis runs over, the one named last changes fastest.
Arguments:
- tokens: bfloat16 [6144, 2048], P('fs'), may hold values from -6 to 6
- norm_gain: float32 [2048], P('fs'), may hold values from 0.1 to 1.9
- expert_gate: float32 [64, 2048, 1024], P(None, 'fs', 'tp'), may hold values from -0.125 to 0.125
- expert_up: float32 [64, 2048, 1024], P(None, 'fs', 'tp'), may hold values from -0.125 to 0.125
- expert_down: float32 [64, 1024, 2048], P(None, 'fs', 'tp'), may hold values from -0.1875 to 0.1875
- shared_gate: float32 [2048, 1024], P('fs', 'tp'), may hold values from -0.125 to 0.125
- shared_up: float32 [2048, 1024], P('fs', 'tp'), may hold values from -0.125 to 0.125
- shared_down: float32 [1024, 2048], P('fs', 'tp'), may hold values from -0.1875 to 0.1875
- expert_ids: int32 [6144, 8], P('fs'), may hold values from 0 to 63, all different within a row; in each aligned block of 192 rows (0 to 191, 192 to 383, ...) at most 48 rows name the same one
- route_weights: float32 [6144, 8], P('fs'), may hold values from 0.25 to 1
Outputs:
- gate_ready: bfloat16 [64, 2048, 1024], P('fs', None, 'tp')
- up_ready: bfloat16 [64, 2048, 1024], P('fs', None, 'tp')
- down_ready: bfloat16 [64, 1024, 2048], P('fs', None, 'tp')
- shared_gate_ready: bfloat16 [2048, 1024], P(None, 'tp')
- shared_up_ready: bfloat16 [2048, 1024], P(None, 'tp')
- shared_down_ready: bfloat16 [1024, 2048], P(None, 'tp')
- mixed: bfloat16 [6144, 2048], P('fs', 'tp')
Inputs may be any that keep to these rules, and one draw needn't show every extreme that they name: `expert_ids`: each row names 8 different experts. Among the 192 rows of one index of fs no expert is named more than 48 times, and in every draw some expert is named exactly 48 times there.
All inputs are finite; a program needn't handle non-finite values.
Results may differ from a plain program's by a relative error of at most 0.0085.
Values may be sent and summed in bfloat16 or wider, within the bound.
A program may use at most 128 MiB of HBM per device.

v0:
```python
import jax
import jax.numpy as jnp
from jax import lax
from jax.sharding import PartitionSpec as P

TOP_K = 8
EPS = 1e-06


def cut_along(shard, dim, size):
    before, after = (shard.shape[:dim], shard.shape[dim + 1 :])
    return jnp.moveaxis(shard.reshape(*before, size, -1, *after), dim, 0)


def piece_ends(length, count):
    turn = length // count
    if turn >= 8:
        turn -= turn % 8
    return [turn * k for k in range(1, count)]


def in_order(parts, dim):
    parts = jnp.moveaxis(parts, 0, dim)
    shape = parts.shape
    return parts.reshape(*shape[:dim], shape[dim] * shape[dim + 1], *shape[dim + 2 :])


def several_exchanges(shard, axis, pieces, split_dim, concat_dim):
    parts = cut_along(shard, split_dim, lax.axis_size(axis))
    split_at = max(range(1, max(2, parts.ndim - 1)), key=lambda d: parts.shape[d])
    done = []
    for share in jnp.split(parts, piece_ends(parts.shape[split_at], pieces), axis=split_at):
        if share.size:
            done.append(lax.all_to_all(share, axis, split_axis=0, concat_axis=0, tiled=True))
    return in_order(jnp.concatenate(done, axis=split_at), concat_dim)


def side_by_side(arrays, axis, dim, along):
    ends, at = ([], 0)
    for a in arrays[:-1]:
        at += a.shape[along]
        ends.append(at)
    both = jnp.concatenate(arrays, axis=along)
    return tuple(jnp.split(lax.all_gather(both, axis, axis=dim, tiled=True), ends, axis=along))


def turned_gather(arrays, axis, dims):
    turned = [jnp.moveaxis(a, dim, 0) for a, dim in zip(arrays, dims)]
    widths = [t[0].size for t in turned]
    both = jnp.concatenate([t.reshape(-1, w) for t, w in zip(turned, widths)], axis=1)
    result = lax.all_gather(both, axis, axis=0, tiled=True)
    parts = jnp.split(result, [sum(widths[:k]) for k in range(1, len(widths))], axis=1)
    return tuple(
        (
            jnp.moveaxis(b.reshape(-1, *t.shape[1:]), 0, dim)
            for b, t, dim in zip(parts, turned, dims)
        )
    )


def expert_hidden(rows, gate_new, up_new):
    first = jnp.einsum("secn,enf->secf", rows, gate_new, preferred_element_type=jnp.float32)
    second = jnp.einsum("secn,enf->secf", rows, up_new, preferred_element_type=jnp.float32)
    return (jax.nn.silu(first) * second).astype(jnp.bfloat16)


def body(
    tokens,
    norm_gain,
    expert_gate,
    expert_up,
    expert_down,
    shared_gate,
    shared_up,
    shared_down,
    expert_ids,
    route_weights,
):
    groups = lax.axis_size("fs")
    experts = expert_gate.shape[0]
    per_group = experts // groups
    tok_count = tokens.shape[0]
    capacity = 2 * tok_count * TOP_K // experts
    gate_local = (expert_gate * norm_gain[None, :, None]).astype(jnp.bfloat16)
    up_local = (expert_up * norm_gain[None, :, None]).astype(jnp.bfloat16)
    down_local = expert_down.astype(jnp.bfloat16)
    gate_local = gate_local.reshape((groups, per_group) + gate_local.shape[1:])
    up_local = up_local.reshape((groups, per_group) + up_local.shape[1:])
    down_local = down_local.reshape((groups, per_group) + down_local.shape[1:])
    shared_first_local = (shared_gate * norm_gain[:, None]).astype(jnp.bfloat16)
    shared_second_local = (shared_up * norm_gain[:, None]).astype(jnp.bfloat16)
    shared_third_local = shared_down.astype(jnp.bfloat16)
    gate_moved, up_moved = (
        several_exchanges(gate_local, "fs", 2, 0, 2),
        several_exchanges(up_local, "fs", 2, 0, 2),
    )
    gate_ready = gate_moved[0]
    up_ready = up_moved[0]
    shared_gate_ready, shared_up_ready, shared_down_ready = (
        *side_by_side((shared_first_local, shared_second_local), "fs", 0, 1),
        lax.all_gather(shared_third_local, "fs", axis=0, tiled=True),
    )
    wide = tokens.astype(jnp.float32)
    normed = (wide * lax.rsqrt(jnp.mean(wide * wide, axis=-1, keepdims=True) + EPS)).astype(
        jnp.bfloat16
    )
    chosen = expert_ids.reshape(-1)
    onehot = (chosen[:, None] == jnp.arange(experts, dtype=jnp.int32)[None, :]).astype(jnp.int32)
    ranks = jnp.sum(jnp.cumsum(onehot, axis=0) * onehot, axis=1) - 1
    owners = jnp.arange(tok_count * TOP_K, dtype=jnp.int32) // TOP_K
    slot_token = jnp.zeros((experts, capacity), jnp.int32).at[chosen, ranks].set(owners)
    outgoing = normed[slot_token.reshape(-1)].reshape(groups, per_group, capacity, normed.shape[1])
    share = capacity // lax.axis_size("tp")
    mine = lax.dynamic_slice_in_dim(outgoing, lax.axis_index("tp") * share, share, 2)
    arrived = lax.all_to_all(mine, "fs", split_axis=0, concat_axis=0, tiled=True)
    hidden = expert_hidden(lax.all_gather(arrived, "tp", axis=2, tiled=True), gate_ready, up_ready)
    shared_first = jnp.dot(normed, shared_gate_ready, preferred_element_type=jnp.float32)
    shared_second = jnp.dot(normed, shared_up_ready, preferred_element_type=jnp.float32)
    shared_hidden = (jax.nn.silu(shared_first) * shared_second).astype(jnp.bfloat16)[None, None]
    down_moved = lax.all_to_all(down_local, "fs", split_axis=0, concat_axis=2, tiled=True)
    down_ready = down_moved[0]
    columns = down_ready.shape[2]
    routed_piece, shared_piece = turned_gather((hidden, shared_hidden), "tp", (3, 3))
    routed_total = jnp.einsum(
        "secf,efd->secd", routed_piece, down_ready, preferred_element_type=jnp.float32
    )
    shared_total = jnp.einsum(
        "abtf,fd->abtd", shared_piece, shared_down_ready, preferred_element_type=jnp.float32
    )
    returned = lax.all_to_all(
        routed_total.astype(jnp.bfloat16), "fs", split_axis=0, concat_axis=0, tiled=True
    )
    returned = returned.reshape(experts * capacity, columns)
    picked = (
        returned[chosen * capacity + ranks].astype(jnp.float32).reshape(tok_count, TOP_K, columns)
    )
    routed = jnp.sum(picked * route_weights[:, :, None], axis=1)
    mixed = (shared_total[0, 0] + routed).astype(jnp.bfloat16)
    return (
        gate_ready,
        up_ready,
        down_ready,
        shared_gate_ready,
        shared_up_ready,
        shared_down_ready,
        mixed,
    )


def solution(mesh):
    in_specs = (
        P("fs", None),
        P("fs"),
        P(None, "fs", "tp"),
        P(None, "fs", "tp"),
        P(None, "fs", "tp"),
        P("fs", "tp"),
        P("fs", "tp"),
        P("fs", "tp"),
        P("fs", None),
        P("fs", None),
    )
    out_specs = (
        P("fs", None, "tp"),
        P("fs", None, "tp"),
        P("fs", None, "tp"),
        P(None, "tp"),
        P(None, "tp"),
        P(None, "tp"),
        P("fs", "tp"),
    )
    return jax.shard_map(body, mesh=mesh, in_specs=in_specs, out_specs=out_specs, check_vma=False)
```

profile of v0, /device:TPU:32, one launch (start us, length us, event | category | flops | bytes accessed | tf_op | source)
XLA Modules:
  0.0 414.8 jit_solution(16375426263147226016)
XLA Ops:
  8.4 18.1 %reduce-window.6 = s32[64,12,128]{2,1,0:T(8,128)S(1)} reduce-window(s32[64,12,128]{2,1,0:T(8,128)S(1)} %fusion.25, s32[]{:T(128)} %constant.44.clone.1), window={size=1x1x128 pad=0_0x0_0x127_0}, to_apply=%region_1.0 | reduce-window | flops 12484608 | bytes 786436 | tf_op jit(solution)/shard_map/reduce-window
  27.8 6.2 %scatter_custom_fusion = s32[3072]{0:T(1024)S(1)} fusion(s32[1536]{0:T(1024)S(1)} %get-tuple-element.23, s32[1536]{0:T(1024)S(1)} %get-tuple-element.22, s32[]{:T(128)} %constant.44.clone.1), kind=kCustom, calls=%fused_computation.63 | custom fusion | bytes 12292
  34.7 15.9 %gather_fusion = bf16[3072,2048]{1,0:T(8,128)(2,1)} fusion(bf16[192,2048]{1,0:T(8,128)(2,1)S(1)} %fusion.11, s32[3072]{0:T(1024)S(1)} %broadcast_clamp_fusion), kind=kCustom, calls=%fused_computation | custom fusion | bytes 25178112 | tf_op jit(solution)/shard_map/gather | solution.py:112
  50.7 3.0 constant_dynamic-slice_fusion
  53.7 2.8 copy.64
  56.5 11.3 %all-to-all-start.5 = ((bf16[32,2,6,2048]{3,1,2,0:T(2,128)(2,1)}), bf16[32,2,6,2048]{3,1,2,0:T(2,128)(2,1)S(1)}, u32[]{:S(2)}, u32[]{:S(2)}) async-start(bf16[32,2,6,2048]{3,1,2,0:T(2,128)(2,1)} %copy.64), calls=%async_computation.5 | async-start | bytes 3145728 | tf_op jit(solution)/shard_map/all_to_all | solution.py:115
  68.6 38.4 %all-to-all-done.5 = bf16[32,2,6,2048]{3,1,2,0:T(2,128)(2,1)S(1)} async-done(((bf16[32,2,6,2048]{3,1,2,0:T(2,128)(2,1)}), bf16[32,2,6,2048]{3,1,2,0:T(2,128)(2,1)S(1)}, u32[]{:S(2)}, u32[]{:S(2)}) %all-to-all-start.5) | async-done | bytes 1572896 | tf_op jit(solution)/shard_map/all_to_all | solution.py:115
  107.1 2.0 copy.65
  109.1 2.8 multiply_convert_fusion
  112.0 0.9 fusion.36
  112.9 23.9 %all_to_all.45 = bf16[32,1,2,32,128]{4,3,2,1,0:T(8,128)(2,1)S(1)} all-to-all(bf16[32,1,2,32,128]{4,3,2,1,0:T(8,128)(2,1)S(1)} %get-tuple-element.11), channel_id=1, replica_groups=mesh['fs'=32,'tp'=8] {'fs'}, dimensions={0} | all-to-all | bytes 1048576 | tf_op jit(solution)/shard_map/all_to_all | solution.py:34
  136.8 5.0 %all-to-all-start.1 = ((bf16[32,1,2,32,128]{4,3,2,1,0:T(8,128)(2,1)}), bf16[32,1,2,32,128]{4,3,2,1,0:T(8,128)(2,1)S(1)}, u32[]{:S(2)}, u32[]{:S(2)}) async-start(bf16[32,1,2,32,128]{4,3,2,1,0:T(8,128)(2,1)} %get-tuple-element.12), calls=%async_computation.1 | async-start | bytes 1048576 | tf_op jit(solution)/shard_map/all_to_all | solution.py:34
  141.8 0.9 fusion.35
  142.8 15.6 %all-to-all-done.1 = bf16[32,1,2,32,128]{4,3,2,1,0:T(8,128)(2,1)S(1)} async-done(((bf16[32,1,2,32,128]{4,3,2,1,0:T(8,128)(2,1)}), bf16[32,1,2,32,128]{4,3,2,1,0:T(8,128)(2,1)S(1)}, u32[]{:S(2)}, u32[]{:S(2)}) %all-to-all-start.1) | async-done | bytes 524320 | tf_op jit(solution)/shard_map/all_to_all | solution.py:34
  158.4 21.5 %all_to_all.46 = bf16[32,1,2,32,128]{4,3,2,1,0:T(8,128)(2,1)S(1)} all-to-all(bf16[32,1,2,32,128]{4,3,2,1,0:T(8,128)(2,1)S(1)} %get-tuple-element.9), channel_id=1, replica_groups=mesh['fs'=32,'tp'=8] {'fs'}, dimensions={0} | all-to-all | bytes 1048576 | tf_op jit(solution)/shard_map/all_to_all | solution.py:34
  179.9 5.1 %all-to-all-start.3 = ((bf16[32,1,2,32,128]{4,3,2,1,0:T(8,128)(2,1)}), bf16[32,1,2,32,128]{4,3,2,1,0:T(8,128)(2,1)S(1)}, u32[]{:S(2)}, u32[]{:S(2)}) async-start(bf16[32,1,2,32,128]{4,3,2,1,0:T(8,128)(2,1)} %get-tuple-element.10), calls=%async_computation.3 | async-start | bytes 1048576 | tf_op jit(solution)/shard_map/all_to_all | solution.py:34
  185.5 16.0 %all-to-all-done.3 = bf16[32,1,2,32,128]{4,3,2,1,0:T(8,128)(2,1)S(1)} async-done(((bf16[32,1,2,32,128]{4,3,2,1,0:T(8,128)(2,1)}), bf16[32,1,2,32,128]{4,3,2,1,0:T(8,128)(2,1)S(1)}, u32[]{:S(2)}, u32[]{:S(2)}) %all-to-all-start.3) | async-done | bytes 524320 | tf_op jit(solution)/shard_map/all_to_all | solution.py:34
  201.7 1.6 fusion.34
  204.5 18.0 %all-gather.6.cloned.1.call-done = bf16[32,2,48,2048]{3,0,1,2:T(8,128)(2,1)} async-done(((bf16[32,2,6,2048]{3,0,1,2:T(8,128)(2,1)}), bf16[32,2,48,2048]{3,0,1,2:T(8,128)(2,1)}) %all-gather.6.cloned.1.call-update) | async-done | bytes 12582928 | tf_op jit(solution)/shard_map/all_gather | solution.py:116
  222.5 18.0 %fusion.2 = f32[2,128,32,48]{1,3,2,0:T(8,128)S(1)} fusion(bf16[2,2048,128,1]{2,1,3,0:T(8,128)(2,1)S(1)} %bitcast.105, bf16[32,2,48,2048]{3,0,1,2:T(8,128)(2,1)} %all-gather.6.cloned.1.call-done), kind=kOutput, calls=%fused_computation.5 | convolution fusion | flops 1610612736 | bytes 15204352 | tf_op jit(solution)/shard_map/secn,enf->secf/dot_general | solution.py:62
  240.6 13.8 %fusion.13 = bf16[128,32,2,48]{0,3,1,2:T(8,128)(2,1)S(1)} fusion(f32[2,128,32,48]{1,3,2,0:T(8,128)S(1)} %fusion.2, bf16[2,2048,128,1]{2,1,3,0:T(8,128)(2,1)S(1)} %bitcast.107, bf16[32,2,48,2048]{3,0,1,2:T(8,128)(2,1)} %all-gather.6.cloned.1.call-done), kind=kOutput, calls=%fused_computation.20 | convolution fusion | flops 1612972032 | bytes 15990784 | tf_op jit(solution)/shard_map/secn,enf->secf/dot_general | solution.py:63
  254.4 0.9 pad_maximum_fusion
  255.4 0.9 copy-done.1
  256.4 37.4 %all_to_all.47 = bf16[32,2,32,256]{3,2,1,0:T(8,128)(2,1)S(1)} all-to-all(bf16[32,2,32,256]{3,2,1,0:T(8,128)(2,1)S(1)} %bitcast.101), channel_id=1, replica_groups=mesh['fs'=32,'tp'=8] {'fs'}, dimensions={0} | all-to-all | bytes 2097152 | tf_op jit(solution)/shard_map/all_to_all | solution.py:120
  293.9 10.6 %all-gather.8.cloned.1.call-done = bf16[1024,3264]{0,1:T(8,128)(2,1)} async-done(((bf16[128,3264]{0,1:T(8,128)(2,1)}), bf16[1024,3264]{0,1:T(8,128)(2,1)}) %all-gather.8.cloned.1.call-update) | async-done | bytes 6684688 | tf_op jit(solution)/shard_map/all_gather | solution.py:51
  304.6 2.8 slice-done
  307.4 1.8 fusion.17
  309.2 1.4 copy.70
  310.6 10.2 %all-to-all-start.6 = ((bf16[32,2,48,256]{3,2,1,0:T(8,128)(2,1)}), bf16[32,2,48,256]{3,2,1,0:T(8,128)(2,1)S(1)}, u32[]{:S(2)}, u32[]{:S(2)}) async-start(bf16[32,2,48,256]{3,2,1,0:T(8,128)(2,1)} %copy.70), calls=%async_computation.6 | async-start | bytes 3145728 | tf_op jit(solution)/shard_map/all_to_all | solution.py:130
  320.9 79.3 %all_gather.13 = bf16[1024,256]{1,0:T(8,128)(2,1)S(1)} all-gather(bf16[32,256]{1,0:T(8,128)(2,1)S(1)} %convert_element_type.57), channel_id=1, replica_groups=mesh['fs'=32,'tp'=8] {'fs'}, dimensions={0}, use_global_device_ids=true | all-gather | bytes 540672 | tf_op jit(solution)/shard_map/all_gather | solution.py:101
  400.3 4.8 %gather_fusion.1 = bf16[1536,256]{1,0:T(8,128)(2,1)S(1)} fusion(bf16[3072,256]{1,0:T(8,128)(2,1)S(1)} %bitcast.96, s32[2048]{0:T(1024)S(1)} %pad_clamp_fusion), kind=kCustom, calls=%fused_computation.1 | custom fusion | bytes 1579008 | tf_op jit(solution)/shard_map/gather | solution.py:135
  405.6 1.9 fusion.22
  (76 shorter events, 7.4 us)
Async XLA Ops:
  8.3 19.2 %copy-start.13 = (s32[2]{0:T(128)S(1)}, s32[2]{0:T(128)}, u32[]{:S(2)}) copy-start(s32[2]{0:T(128)} %constant.57) | copy-start | bytes 28
  8.4 19.3 %copy-start.12 = (s32[2]{0:T(128)S(1)}, s32[2]{0:T(128)}, u32[]{:S(2)}) copy-start(s32[2]{0:T(128)} %constant.60) | copy-start | bytes 28
  8.4 25.9 %copy-start = (bf16[192,2048]{1,0:T(8,128)(2,1)S(1)}, bf16[192,2048]{1,0:T(8,128)(2,1)}, u32[]{:S(2)}) copy-start(bf16[192,2048]{1,0:T(8,128)(2,1)} %param.10) | copy-start | bytes 2359300
  56.5 11.4 %copy-start.7 = (f32[64,128]{1,0:T(8,128)S(1)}, f32[64,128]{1,0:T(8,128)}, u32[]{:S(2)}) copy-start(f32[64,128]{1,0:T(8,128)} %param.15) | copy-start | bytes 98308
  56.5 11.4 %copy-start.8 = (f32[64,128]{1,0:T(8,128)S(1)}, f32[64,128]{1,0:T(8,128)}, u32[]{:S(2)}) copy-start(f32[64,128]{1,0:T(8,128)} %param.16) | copy-start | bytes 98308
  56.5 11.4 %copy-start.11 = (f32[64]{0:T(128)S(1)}, f32[64]{0:T(128)}, u32[]{:S(2)}) copy-start(f32[64]{0:T(128)} %param.11) | copy-start | bytes 772
  56.5 50.6 %all-to-all-start.5 = ((bf16[32,2,6,2048]{3,1,2,0:T(2,128)(2,1)}), bf16[32,2,6,2048]{3,1,2,0:T(2,128)(2,1)S(1)}, u32[]{:S(2)}, u32[]{:S(2)}) async-start(bf16[32,2,6,2048]{3,1,2,0:T(2,128)(2,1)} %copy.64), calls=%async_computation.5 | async-start | bytes 3145728 | tf_op jit(solution)/shard_map/all_to_all | solution.py:115
  67.8 133.9 %all-gather.4.cloned.1.call-start = ((), (), s32[]{:S(2)}) async-start(), calls=%async_computation.7 | async-start | bytes 1081344 | tf_op jit(solution)/shard_map/all_gather | solution.py:44
  68.6 153.9 %all-gather.6.cloned.1.call-start = ((), (), s32[]{:S(2)}) async-start(), calls=%async_computation.8 | async-start | bytes 14155776 | tf_op jit(solution)/shard_map/all_gather | solution.py:116
  136.8 21.6 %all-to-all-start.1 = ((bf16[32,1,2,32,128]{4,3,2,1,0:T(8,128)(2,1)}), bf16[32,1,2,32,128]{4,3,2,1,0:T(8,128)(2,1)S(1)}, u32[]{:S(2)}, u32[]{:S(2)}) async-start(bf16[32,1,2,32,128]{4,3,2,1,0:T(8,128)(2,1)} %get-tuple-element.12), calls=%async_computation.1 | async-start | bytes 1048576 | tf_op jit(solution)/shard_map/all_to_all | solution.py:34
  179.9 21.5 %all-to-all-start.3 = ((bf16[32,1,2,32,128]{4,3,2,1,0:T(8,128)(2,1)}), bf16[32,1,2,32,128]{4,3,2,1,0:T(8,128)(2,1)S(1)}, u32[]{:S(2)}, u32[]{:S(2)}) async-start(bf16[32,1,2,32,128]{4,3,2,1,0:T(8,128)(2,1)} %get-tuple-element.10), calls=%async_computation.3 | async-start | bytes 1048576 | tf_op jit(solution)/shard_map/all_to_all | solution.py:34
  185.0 119.6 %all-gather.8.cloned.1.call-start = ((), (), s32[]{:S(2)}) async-start(), calls=%async_computation.9 | async-start | bytes 7520256 | tf_op jit(solution)/shard_map/all_gather | solution.py:51
  185.4 37.0 %copy-start.3 = (bf16[1,2,32,64,128]{4,3,2,1,0:T(8,128)(2,1)}, bf16[1,2,32,64,128]{4,3,2,1,0:T(8,128)(2,1)S(1)}, u32[]{:S(2)}) copy-start(bf16[1,2,32,64,128]{4,3,2,1,0:T(8,128)(2,1)S(1)} %copy.55) | copy-start | bytes 3145732
  201.6 38.9 %copy-start.4 = (bf16[1,2,32,64,128]{4,3,2,1,0:T(8,128)(2,1)}, bf16[1,2,32,64,128]{4,3,2,1,0:T(8,128)(2,1)S(1)}, u32[]{:S(2)}) copy-start(bf16[1,2,32,64,128]{4,3,2,1,0:T(8,128)(2,1)S(1)} %copy.56) | copy-start | bytes 3145732
  203.3 0.8 copy-start.6
  203.3 37.2 %copy-start.2 = (bf16[2048,128]{1,0:T(8,128)(2,1)}, bf16[2048,128]{1,0:T(8,128)(2,1)S(1)}, u32[]{:S(2)}) copy-start(bf16[2048,128]{1,0:T(8,128)(2,1)S(1)} %get-tuple-element.34) | copy-start | bytes 1572868
  254.3 1.9 copy-start.1
  293.9 10.7 %copy-start.5 = (bf16[1,2,32,32,256]{4,3,2,1,0:T(8,128)(2,1)}, bf16[1,2,32,32,256]{4,3,2,1,0:T(8,128)(2,1)S(1)}, u32[]{:S(2)}) copy-start(bf16[1,2,32,32,256]{4,3,2,1,0:T(8,128)(2,1)S(1)} %copy.57) | copy-start | bytes 3145732
  304.6 2.8 slice-start
  310.6 10.2 %copy-start.10 = (f32[192,8]{0,1:T(8,128)S(1)}, f32[192,8]{0,1:T(8,128)}, u32[]{:S(2)}) copy-start(f32[192,8]{0,1:T(8,128)} %param.19) | copy-start | bytes 18436
  310.6 10.3 %copy-start.9 = (f32[32,256]{1,0:T(8,128)S(1)}, f32[32,256]{1,0:T(8,128)}, u32[]{:S(2)}) copy-start(f32[32,256]{1,0:T(8,128)} %param.17) | copy-start | bytes 98308
  310.6 89.7 %all-to-all-start.6 = ((bf16[32,2,48,256]{3,2,1,0:T(8,128)(2,1)}), bf16[32,2,48,256]{3,2,1,0:T(8,128)(2,1)S(1)}, u32[]{:S(2)}, u32[]{:S(2)}) async-start(bf16[32,2,48,256]{3,2,1,0:T(8,128)(2,1)} %copy.70), calls=%async_computation.6 | async-start | bytes 3145728 | tf_op jit(solution)/shard_map/all_to_all | solution.py:130
Sparse Core Ops, SparseCore 0:
  71.8 80.5 all-gather.3
  154.2 68.2 all-gather.5
  255.5 49.0 all-gather.7
where the time goes:
time: 416 us; the launch traced here: 415 us
  blocking collectives  162 us (39%)
  waiting for transfers between devices  98.7 us (24%)
  local copies, waits for them, and re-layouts  46.8 us (11%)
  matrix products  36.3 us (9%)
  starting transfers between devices  31.9 us (8%)
  other arithmetic  24.6 us (6%)
  between operations  14.2 us (3%)
    all_gather x1, blocking collectives, body(): lax.all_gather(shared_third_local, 'fs', axis=0, tiled=True)  79.3 us
    all_to_all x2, blocking collectives, several_exchanges(): lax.all_to_all(share, axis, split_axis=0, concat_axis=0, tiled=True)  45.4 us
    all_to_all x1, waiting for transfers between devices, body(): lax.all_to_all(mine, 'fs', split_axis=0, concat_axis=0, tiled=True)  38.4 us
    all_to_all x1, blocking collectives, body(): lax.all_to_all(down_local, 'fs', split_axis=0, concat_axis=2, tiled=True)  37.4 us
    all_to_all x2, waiting for transfers between devices, several_exchanges(): lax.all_to_all(share, axis, split_axis=0, concat_axis=0, tiled=True)  31.6 us
    another operation x3, other arithmetic  18.4 us
    dot_general x1, matrix products, expert_hidden(): jnp.einsum('secn,enf->secf', rows, gate_new, preferred_element_type=jnp.f...  18 us
    all_gather x1, waiting for transfers between devices, body(): lax.all_gather(arrived, 'tp', axis=2, tiled=True)  18 us
  transfers between devices with their start and end apart: 7, of which 5 were waited for; matrix products, arithmetic and copies ran while one was open for 3% of the time, Pallas kernels for 0%

commit v1 on v0

--- a/solution.py
+++ b/solution.py
@@ -5,6 +5,11 @@
 
 TOP_K = 8
 EPS = 1e-06
+
+
+def tiled_gather(x, axis, dim):
+    copies = jnp.concatenate([x] * lax.axis_size(axis), axis=dim)
+    return lax.all_to_all(copies, axis, dim, dim, tiled=True)
 
 
 def cut_along(shard, dim, size):
@@ -98,7 +103,7 @@
     up_ready = up_moved[0]
     shared_gate_ready, shared_up_ready, shared_down_ready = (
         *side_by_side((shared_first_local, shared_second_local), "fs", 0, 1),
-        lax.all_gather(shared_third_local, "fs", axis=0, tiled=True),
+        tiled_gather(shared_third_local, "fs", 0),
     )
     wide = tokens.astype(jnp.float32)
     normed = (wide * lax.rsqrt(jnp.mean(wide * wide, axis=-1, keepdims=True) + EPS)).astype(

time: 416 us -> 377 us (0.906)
  blocking collectives: 162 us -> 45.4 us
  waiting for transfers between devices: 98.7 us -> 144 us
  local copies, waits for them, and re-layouts: 46.8 us -> 65.7 us
  starting transfers between devices: 31.9 us -> 43.4 us
    all_gather x1 -> x0, blocking collectives: 79.3 us -> none  [body(): lax.all_gather(shared_third_local, 'fs', axis=0, tiled=True)]
    all_to_all x1 -> x0, blocking collectives: 37.4 us -> none  [body(): lax.all_to_all(down_local, 'fs', split_axis=0, concat_axis=2, tiled=True)]
    all_to_all x1, waiting for transfers between devices: 0.01 us -> 37.2 us  [body(): lax.all_to_all(routed_total.astype(jnp.bfloat16), 'fs', split_axis=0, con...]
    unnamed x33 -> x63, local copies, waits for them, and re-layouts: 9.3 us -> 27.5 us
    all_to_all x0 -> x2, starting transfers between devices: none -> 16.5 us  [the longest x1 10.1 us: body(): lax.all_to_all(down_local, 'fs', split_axis=0, concat_axis=2, tiled=True)]
    all_to_all x0 -> x2, waiting for transfers between devices: none -> 15.3 us  [the longest x1 8.16 us: body(): lax.all_to_all(down_local, 'fs', split_axis=0, concat_axis=2, tiled=True)]
    all_gather x1, waiting for transfers between devices: 10.6 us -> 3 us  [turned_gather(): result = lax.all_gather(both, axis, axis=0, tiled=True)]
    all_to_all x1, starting transfers between devices: 10.2 us -> 5.12 us  [body(): lax.all_to_all(routed_total.astype(jnp.bfloat16), 'fs', split_axis=0, con...]
  transfers between devices with their start and end apart: 7 -> 9, of which waited for: 5 -> 8; matrix products, arithmetic and copies ran while one was open for 3% -> 9% of each run, Pallas kernels for 0% -> 0%
where the time goes in v1:
time: 377 us; the launch traced here: 375 us
  waiting for transfers between devices  144 us (38%)
  local copies, waits for them, and re-layouts  65.7 us (17%)
  blocking collectives  45.4 us (12%)
  starting transfers between devices  43.4 us (12%)
  matrix products  36.3 us (10%)
  other arithmetic  26.2 us (7%)
  between operations  14.2 us (4%)
    all_to_all x2, blocking collectives, several_exchanges(): lax.all_to_all(share, axis, split_axis=0, concat_axis=0, tiled=True)  45.4 us
    all_to_all x1, waiting for transfers between devices, body(): lax.all_to_all(mine, 'fs', split_axis=0, concat_axis=0, tiled=True)  38.4 us
    all_to_all x1, waiting for transfers between devices, body(): lax.all_to_all(routed_total.astype(jnp.bfloat16), 'fs', split_axis=0, con...  37.2 us
    all_to_all x2, waiting for transfers between devices, several_exchanges(): lax.all_to_all(share, axis, split_axis=0, concat_axis=0, tiled=True)  31.6 us
    unnamed x63, local copies, waits for them, and re-layouts  27.5 us
    another operation x3, other arithmetic  18.4 us
    dot_general x1, matrix products, expert_hidden(): jnp.einsum('secn,enf->secf', rows, gate_new, preferred_element_type=jnp.f...  18 us
    all_gather x1, waiting for transfers between devices, body(): lax.all_gather(arrived, 'tp', axis=2, tiled=True)  18 us
  transfers between devices with their start and end apart: 9, of which 8 were waited for; matrix products, arithmetic and copies ran while one was open for 9% of the time, Pallas kernels for 0%

profile of v1, /device:TPU:32, one launch (start us, length us, event | category | flops | bytes accessed | tf_op | source)
XLA Modules:
  0.0 374.8 jit_solution(3604918386813535641)
XLA Ops:
  8.4 18.1 %reduce-window.6 = s32[64,12,128]{2,1,0:T(8,128)S(1)} reduce-window(s32[64,12,128]{2,1,0:T(8,128)S(1)} %fusion.25, s32[]{:T(128)} %constant.44.clone.1), window={size=1x1x128 pad=0_0x0_0x127_0}, to_apply=%region_1.0 | reduce-window | flops 12484608 | bytes 786436 | tf_op jit(solution)/shard_map/reduce-window
  27.8 6.2 %scatter_custom_fusion = s32[3072]{0:T(1024)S(1)} fusion(s32[1536]{0:T(1024)S(1)} %get-tuple-element.25, s32[1536]{0:T(1024)S(1)} %get-tuple-element.24, s32[]{:T(128)} %constant.44.clone.1), kind=kCustom, calls=%fused_computation.95 | custom fusion | bytes 12292
  34.7 15.9 %gather_fusion = bf16[3072,2048]{1,0:T(8,128)(2,1)} fusion(bf16[192,2048]{1,0:T(8,128)(2,1)S(1)} %fusion.11, s32[3072]{0:T(1024)S(1)} %broadcast_clamp_fusion), kind=kCustom, calls=%fused_computation | custom fusion | bytes 25178112 | tf_op jit(solution)/shard_map/gather | solution.py:117
  50.7 3.0 constant_dynamic-slice_fusion
  53.7 2.8 copy.64
  56.5 11.3 %all-to-all-start.6 = ((bf16[32,2,6,2048]{3,1,2,0:T(2,128)(2,1)}), bf16[32,2,6,2048]{3,1,2,0:T(2,128)(2,1)S(1)}, u32[]{:S(2)}, u32[]{:S(2)}) async-start(bf16[32,2,6,2048]{3,1,2,0:T(2,128)(2,1)} %copy.64), calls=%async_computation.6 | async-start | bytes 3145728 | tf_op jit(solution)/shard_map/all_to_all | solution.py:120
  68.7 38.4 %all-to-all-done.6 = bf16[32,2,6,2048]{3,1,2,0:T(2,128)(2,1)S(1)} async-done(((bf16[32,2,6,2048]{3,1,2,0:T(2,128)(2,1)}), bf16[32,2,6,2048]{3,1,2,0:T(2,128)(2,1)S(1)}, u32[]{:S(2)}, u32[]{:S(2)}) %all-to-all-start.6) | async-done | bytes 1572896 | tf_op jit(solution)/shard_map/all_to_all | solution.py:120
  107.1 2.0 copy.65
  109.2 2.8 multiply_convert_fusion
  112.9 23.9 %all_to_all.57 = bf16[32,1,2,32,128]{4,3,2,1,0:T(8,128)(2,1)S(1)} all-to-all(bf16[32,1,2,32,128]{4,3,2,1,0:T(8,128)(2,1)S(1)} %get-tuple-element.13), channel_id=1, replica_groups=mesh['fs'=32,'tp'=8] {'fs'}, dimensions={0} | all-to-all | bytes 1048576 | tf_op jit(solution)/shard_map/all_to_all | solution.py:39
  136.8 5.0 %all-to-all-start.1 = ((bf16[32,1,2,32,128]{4,3,2,1,0:T(8,128)(2,1)}), bf16[32,1,2,32,128]{4,3,2,1,0:T(8,128)(2,1)S(1)}, u32[]{:S(2)}, u32[]{:S(2)}) async-start(bf16[32,1,2,32,128]{4,3,2,1,0:T(8,128)(2,1)} %get-tuple-element.14), calls=%async_computation.1 | async-start | bytes 1048576 | tf_op jit(solution)/shard_map/all_to_all | solution.py:39
  142.8 15.6 %all-to-all-done.1 = bf16[32,1,2,32,128]{4,3,2,1,0:T(8,128)(2,1)S(1)} async-done(((bf16[32,1,2,32,128]{4,3,2,1,0:T(8,128)(2,1)}), bf16[32,1,2,32,128]{4,3,2,1,0:T(8,128)(2,1)S(1)}, u32[]{:S(2)}, u32[]{:S(2)}) %all-to-all-start.1) | async-done | bytes 524320 | tf_op jit(solution)/shard_map/all_to_all | solution.py:39
  158.4 21.5 %all_to_all.58 = bf16[32,1,2,32,128]{4,3,2,1,0:T(8,128)(2,1)S(1)} all-to-all(bf16[32,1,2,32,128]{4,3,2,1,0:T(8,128)(2,1)S(1)} %get-tuple-element.11), channel_id=1, replica_groups=mesh['fs'=32,'tp'=8] {'fs'}, dimensions={0} | all-to-all | bytes 1048576 | tf_op jit(solution)/shard_map/all_to_all | solution.py:39
  179.9 5.1 %all-to-all-start.3 = ((bf16[32,1,2,32,128]{4,3,2,1,0:T(8,128)(2,1)}), bf16[32,1,2,32,128]{4,3,2,1,0:T(8,128)(2,1)S(1)}, u32[]{:S(2)}, u32[]{:S(2)}) async-start(bf16[32,1,2,32,128]{4,3,2,1,0:T(8,128)(2,1)} %get-tuple-element.12), calls=%async_computation.3 | async-start | bytes 1048576 | tf_op jit(solution)/shard_map/all_to_all | solution.py:39
  185.5 16.0 %all-to-all-done.3 = bf16[32,1,2,32,128]{4,3,2,1,0:T(8,128)(2,1)S(1)} async-done(((bf16[32,1,2,32,128]{4,3,2,1,0:T(8,128)(2,1)}), bf16[32,1,2,32,128]{4,3,2,1,0:T(8,128)(2,1)S(1)}, u32[]{:S(2)}, u32[]{:S(2)}) %all-to-all-start.3) | async-done | bytes 524320 | tf_op jit(solution)/shard_map/all_to_all | solution.py:39
  201.7 1.6 fusion.34
  204.5 18.0 %all-gather.6.cloned.1.call-done = bf16[32,2,48,2048]{3,0,1,2:T(8,128)(2,1)} async-done(((bf16[32,2,6,2048]{3,0,1,2:T(8,128)(2,1)}), bf16[32,2,48,2048]{3,0,1,2:T(8,128)(2,1)}) %all-gather.6.cloned.1.call-update) | async-done | bytes 12582928 | tf_op jit(solution)/shard_map/all_gather | solution.py:121
  222.5 18.0 %fusion.2 = f32[2,128,32,48]{1,3,2,0:T(8,128)S(1)} fusion(bf16[2,2048,128,1]{2,1,3,0:T(8,128)(2,1)S(1)} %bitcast.108, bf16[32,2,48,2048]{3,0,1,2:T(8,128)(2,1)} %all-gather.6.cloned.1.call-done), kind=kOutput, calls=%fused_computation.5 | convolution fusion | flops 1610612736 | bytes 15204352 | tf_op jit(solution)/shard_map/secn,enf->secf/dot_general | solution.py:67
  240.6 13.8 %fusion.13 = bf16[128,32,2,48]{0,3,1,2:T(8,128)(2,1)S(1)} fusion(f32[2,128,32,48]{1,3,2,0:T(8,128)S(1)} %fusion.2, bf16[2,2048,128,1]{2,1,3,0:T(8,128)(2,1)S(1)} %bitcast.110, bf16[32,2,48,2048]{3,0,1,2:T(8,128)(2,1)} %all-gather.6.cloned.1.call-done), kind=kOutput, calls=%fused_computation.20 | convolution fusion | flops 1612972032 | bytes 15990784 | tf_op jit(solution)/shard_map/secn,enf->secf/dot_general | solution.py:68
  256.2 1.1 convert_element_type.54
  257.4 10.1 %all-to-all-start.4 = ((bf16[32,2,32,256]{3,2,1,0:T(8,128)(2,1)}), bf16[32,2,32,256]{3,2,1,0:T(8,128)(2,1)S(1)}, u32[]{:S(2)}, u32[]{:S(2)}) async-start(bf16[32,2,32,256]{3,2,1,0:T(8,128)(2,1)} %bitcast.6), calls=%async_computation.4 | async-start | bytes 2097152 | tf_op jit(solution)/shard_map/all_to_all | solution.py:125
  286.9 8.2 %all-to-all-done.4 = bf16[32,2,32,256]{3,2,1,0:T(8,128)(2,1)S(1)} async-done(((bf16[32,2,32,256]{3,2,1,0:T(8,128)(2,1)}), bf16[32,2,32,256]{3,2,1,0:T(8,128)(2,1)S(1)}, u32[]{:S(2)}, u32[]{:S(2)}) %all-to-all-start.4) | async-done | bytes 1048608 | tf_op jit(solution)/shard_map/all_to_all | solution.py:125
  295.0 6.5 %all-to-all-start.5 = ((bf16[32,32,256]{2,1,0:T(8,128)(2,1)}), bf16[32,32,256]{2,1,0:T(8,128)(2,1)S(1)}, u32[]{:S(2)}, u32[]{:S(2)}) async-start(bf16[32,32,256]{2,1,0:T(8,128)(2,1)} %bitcast.10), calls=%async_computation.5 | async-start | bytes 1048576 | tf_op jit(solution)/shard_map/all_to_all | solution.py:12
  301.6 3.0 all-gather.8.cloned.1.call-done
  304.6 2.8 slice-done
  307.4 1.8 fusion.17
  309.2 1.4 copy.70
  310.6 7.2 %all-to-all-done.5 = bf16[32,32,256]{2,1,0:T(8,128)(2,1)S(1)} async-done(((bf16[32,32,256]{2,1,0:T(8,128)(2,1)}), bf16[32,32,256]{2,1,0:T(8,128)(2,1)S(1)}, u32[]{:S(2)}, u32[]{:S(2)}) %all-to-all-start.5) | async-done | bytes 524320 | tf_op jit(solution)/shard_map/all_to_all | solution.py:12
  317.8 5.1 %all-to-all-start.7 = ((bf16[32,2,48,256]{3,2,1,0:T(8,128)(2,1)}), bf16[32,2,48,256]{3,2,1,0:T(8,128)(2,1)S(1)}, u32[]{:S(2)}, u32[]{:S(2)}) async-start(bf16[32,2,48,256]{3,2,1,0:T(8,128)(2,1)} %copy.70), calls=%async_computation.7 | async-start | bytes 3145728 | tf_op jit(solution)/shard_map/all_to_all | solution.py:135
  323.1 37.2 %all-to-all-done.7 = bf16[32,2,48,256]{3,2,1,0:T(8,128)(2,1)S(1)} async-done(((bf16[32,2,48,256]{3,2,1,0:T(8,128)(2,1)}), bf16[32,2,48,256]{3,2,1,0:T(8,128)(2,1)S(1)}, u32[]{:S(2)}, u32[]{:S(2)}) %all-to-all-start.7) | async-done | bytes 1572896 | tf_op jit(solution)/shard_map/all_to_all | solution.py:135
  360.3 4.8 %gather_fusion.1 = bf16[1536,256]{1,0:T(8,128)(2,1)S(1)} fusion(bf16[3072,256]{1,0:T(8,128)(2,1)S(1)} %bitcast.98, s32[2048]{0:T(1024)S(1)} %pad_clamp_fusion), kind=kCustom, calls=%fused_computation.1 | custom fusion | bytes 1579008 | tf_op jit(solution)/shard_map/gather | solution.py:140
  365.6 1.9 fusion.22
  (109 shorter events, 30.4 us)
Async XLA Ops:
  8.3 19.2 %copy-start.13 = (s32[2]{0:T(128)S(1)}, s32[2]{0:T(128)}, u32[]{:S(2)}) copy-start(s32[2]{0:T(128)} %constant.57) | copy-start | bytes 28
  8.4 19.3 %copy-start.12 = (s32[2]{0:T(128)S(1)}, s32[2]{0:T(128)}, u32[]{:S(2)}) copy-start(s32[2]{0:T(128)} %constant.60) | copy-start | bytes 28
  8.4 25.9 %copy-start = (bf16[192,2048]{1,0:T(8,128)(2,1)S(1)}, bf16[192,2048]{1,0:T(8,128)(2,1)}, u32[]{:S(2)}) copy-start(bf16[192,2048]{1,0:T(8,128)(2,1)} %param.10) | copy-start | bytes 2359300
  56.5 11.4 %copy-start.7 = (f32[64,128]{1,0:T(8,128)S(1)}, f32[64,128]{1,0:T(8,128)}, u32[]{:S(2)}) copy-start(f32[64,128]{1,0:T(8,128)} %param.15) | copy-start | bytes 98308
  56.5 11.4 %copy-start.8 = (f32[64,128]{1,0:T(8,128)S(1)}, f32[64,128]{1,0:T(8,128)}, u32[]{:S(2)}) copy-start(f32[64,128]{1,0:T(8,128)} %param.16) | copy-start | bytes 98308
  56.5 11.4 %copy-start.11 = (f32[64]{0:T(128)S(1)}, f32[64]{0:T(128)}, u32[]{:S(2)}) copy-start(f32[64]{0:T(128)} %param.11) | copy-start | bytes 772
  56.5 50.6 %all-to-all-start.6 = ((bf16[32,2,6,2048]{3,1,2,0:T(2,128)(2,1)}), bf16[32,2,6,2048]{3,1,2,0:T(2,128)(2,1)S(1)}, u32[]{:S(2)}, u32[]{:S(2)}) async-start(bf16[32,2,6,2048]{3,1,2,0:T(2,128)(2,1)} %copy.64), calls=%async_computation.6 | async-start | bytes 3145728 | tf_op jit(solution)/shard_map/all_to_all | solution.py:120
  67.8 133.9 %all-gather.4.cloned.1.call-start = ((), (), s32[]{:S(2)}) async-start(), calls=%async_computation.8 | async-start | bytes 1081344 | tf_op jit(solution)/shard_map/all_gather | solution.py:49
  68.6 153.9 %all-gather.6.cloned.1.call-start = ((), (), s32[]{:S(2)}) async-start(), calls=%async_computation.9 | async-start | bytes 14155776 | tf_op jit(solution)/shard_map/all_gather | solution.py:121
  136.8 21.6 %all-to-all-start.1 = ((bf16[32,1,2,32,128]{4,3,2,1,0:T(8,128)(2,1)}), bf16[32,1,2,32,128]{4,3,2,1,0:T(8,128)(2,1)S(1)}, u32[]{:S(2)}, u32[]{:S(2)}) async-start(bf16[32,1,2,32,128]{4,3,2,1,0:T(8,128)(2,1)} %get-tuple-element.14), calls=%async_computation.1 | async-start | bytes 1048576 | tf_op jit(solution)/shard_map/all_to_all | solution.py:39
  179.9 21.5 %all-to-all-start.3 = ((bf16[32,1,2,32,128]{4,3,2,1,0:T(8,128)(2,1)}), bf16[32,1,2,32,128]{4,3,2,1,0:T(8,128)(2,1)S(1)}, u32[]{:S(2)}, u32[]{:S(2)}) async-start(bf16[32,1,2,32,128]{4,3,2,1,0:T(8,128)(2,1)} %get-tuple-element.12), calls=%async_computation.3 | async-start | bytes 1048576 | tf_op jit(solution)/shard_map/all_to_all | solution.py:39
  185.0 119.6 %all-gather.8.cloned.1.call-start = ((), (), s32[]{:S(2)}) async-start(), calls=%async_computation.10 | async-start | bytes 7520256 | tf_op jit(solution)/shard_map/all_gather | solution.py:56
  185.5 37.0 %copy-start.3 = (bf16[1,2,32,64,128]{4,3,2,1,0:T(8,128)(2,1)}, bf16[1,2,32,64,128]{4,3,2,1,0:T(8,128)(2,1)S(1)}, u32[]{:S(2)}) copy-start(bf16[1,2,32,64,128]{4,3,2,1,0:T(8,128)(2,1)S(1)} %copy.55) | copy-start | bytes 3145732
  201.6 38.9 %copy-start.4 = (bf16[1,2,32,64,128]{4,3,2,1,0:T(8,128)(2,1)}, bf16[1,2,32,64,128]{4,3,2,1,0:T(8,128)(2,1)S(1)}, u32[]{:S(2)}) copy-start(bf16[1,2,32,64,128]{4,3,2,1,0:T(8,128)(2,1)S(1)} %copy.56) | copy-start | bytes 3145732
  203.3 0.8 copy-start.6
  203.3 37.2 %copy-start.2 = (bf16[2048,128]{1,0:T(8,128)(2,1)}, bf16[2048,128]{1,0:T(8,128)(2,1)S(1)}, u32[]{:S(2)}) copy-start(bf16[2048,128]{1,0:T(8,128)(2,1)S(1)} %get-tuple-element.36) | copy-start | bytes 1572868
  254.3 1.9 copy-start.1
  256.2 11.2 %copy-start.9 = (f32[32,256]{1,0:T(8,128)S(1)}, f32[32,256]{1,0:T(8,128)}, u32[]{:S(2)}) copy-start(f32[32,256]{1,0:T(8,128)} %param.17) | copy-start | bytes 98308
  257.4 37.7 %all-to-all-start.4 = ((bf16[32,2,32,256]{3,2,1,0:T(8,128)(2,1)}), bf16[32,2,32,256]{3,2,1,0:T(8,128)(2,1)S(1)}, u32[]{:S(2)}, u32[]{:S(2)}) async-start(bf16[32,2,32,256]{3,2,1,0:T(8,128)(2,1)} %bitcast.6), calls=%async_computation.4 | async-start | bytes 2097152 | tf_op jit(solution)/shard_map/all_to_all | solution.py:125
  295.0 22.8 %all-to-all-start.5 = ((bf16[32,32,256]{2,1,0:T(8,128)(2,1)}), bf16[32,32,256]{2,1,0:T(8,128)(2,1)S(1)}, u32[]{:S(2)}, u32[]{:S(2)}) async-start(bf16[32,32,256]{2,1,0:T(8,128)(2,1)} %bitcast.10), calls=%async_computation.5 | async-start | bytes 1048576 | tf_op jit(solution)/shard_map/all_to_all | solution.py:12
  301.6 3.0 copy-start.5
  304.6 2.8 slice-start
  310.6 12.3 %copy-start.10 = (f32[192,8]{0,1:T(8,128)S(1)}, f32[192,8]{0,1:T(8,128)}, u32[]{:S(2)}) copy-start(f32[192,8]{0,1:T(8,128)} %param.19) | copy-start | bytes 18436
  317.8 42.5 %all-to-all-start.7 = ((bf16[32,2,48,256]{3,2,1,0:T(8,128)(2,1)}), bf16[32,2,48,256]{3,2,1,0:T(8,128)(2,1)S(1)}, u32[]{:S(2)}, u32[]{:S(2)}) async-start(bf16[32,2,48,256]{3,2,1,0:T(8,128)(2,1)} %copy.70), calls=%async_computation.7 | async-start | bytes 3145728 | tf_op jit(solution)/shard_map/all_to_all | solution.py:135
Sparse Core Ops, SparseCore 0:
  71.8 80.5 all-gather.3
  154.2 68.2 all-gather.5
  255.5 49.0 all-gather.7
